TPU v7x, 512 devices: a whole 4x8x8 slice. The times are simulated.
512 devices in a mesh: fs: 128 (over z, y, core), tp: 4 (over x).
Axes of the slice: x: 4, y: 8, z: 8, core: 2. Of those that a mesh axis runs over, the one named last changes fastest.
Arguments:
- rnn_out: bfloat16 [98304, 1536], P('fs', 'tp'), may hold values from -6 to 6
- out_grad: bfloat16 [98304, 2048], P('fs', 'tp'), may hold values from -0.078125 to 0.078125
- weight: float32 [2048, 1536], P('fs', 'tp'), may hold values from -0.15625 to 0.15625
- left_root: bfloat16 [4, 2048, 2048], P('tp', 'fs'), as said below
- right_root: bfloat16 [4, 384, 384], P('tp'), as said below
- left_stat: float32 [4, 2048, 2048], P('tp', 'fs'), may hold values from -4 to 4
- right_stat: float32 [4, 384, 384], P('tp', 'fs'), may hold values from -4 to 4
Outputs:
- new_weight: float32 [2048, 1536], P('fs', 'tp')
- step: float32 [2048, 1536], P('fs', 'tp')
- left_new: float32 [4, 2048, 2048], P('tp', 'fs')
- right_new: float32 [4, 384, 384], P('tp', 'fs')
- weight_copy: bfloat16 [2048, 1536], P(None, 'tp')
Inputs may be any that keep to these rules, and one draw needn't show every extreme that they name: `left_root`: each block is symmetric. `right_root`: each block is symmetric.
All inputs are finite; a program needn't handle non-finite values.
Results may differ from a plain program's by a relative error of at most 0.0049.
Values may be sent and summed in bfloat16 or wider, within the bound.
A program may use at most 64 MiB of HBM per device.

v0:
```python
import jax
import jax.numpy as jnp
from jax import lax
from jax.sharding import Mesh
from jax.sharding import PartitionSpec as P

FS = ("fs_0", "fs_1", "fs_2")
FS_TP = ("fs_0", "fs_1", "fs_2", "tp")


decay_rate = 0.8
step_size = 0.005


def by_axis(shard, axes):
    for axis in axes:
        shard = lax.psum(shard, axis)
    return shard


def laid_out(pieces, dim):
    shape = list(pieces.shape[1:])
    shape[dim] *= pieces.shape[0]
    return jnp.moveaxis(pieces, 0, dim).reshape(shape)


def stacked_from(shard, axes, turns):
    pieces = shard[None]
    for k in turns:
        pieces = lax.all_gather(pieces, axes[k], axis=0, tiled=True)
    current = [lax.axis_size(axes[k]) for k in reversed(turns)]
    pieces = pieces.reshape(*current, *shard.shape)
    turned = sorted(range(len(turns)), key=lambda place: turns[len(turns) - 1 - place])
    return pieces.transpose(*turned, *range(len(turns), pieces.ndim)).reshape(-1, *shard.shape)


def gathered_by_axis(shard, axes, turns, dim):
    return laid_out(stacked_from(shard, axes, turns), dim)


def body(rnn_out, out_grad, weight, left_root, right_root, left_stat, right_stat):
    row_count = weight.shape[0]
    block = weight.shape[1]
    width = left_root.shape[2]
    right_rows = right_stat.shape[1]
    right_start = lax.axis_index(FS) * right_rows
    cotangent = lax.all_gather(out_grad, "tp", axis=1, tiled=True)
    whole = lax.psum(
        lax.dot_general(
            cotangent, rnn_out, (((0,), (0,)), ((), ())), preferred_element_type=jnp.float32
        ),
        FS,
    )
    whole_low = whole.astype(jnp.bfloat16)
    grad = lax.dynamic_slice_in_dim(whole, lax.axis_index(FS) * row_count, row_count, 0)
    grad_low = grad.astype(jnp.bfloat16)
    root_columns = left_root[0]
    left_sum = jnp.dot(root_columns, whole_low, preferred_element_type=jnp.float32)
    own_columns = lax.dynamic_slice_in_dim(whole_low, right_start, right_rows, 1)
    right_sum = lax.dot_general(
        own_columns, whole_low, (((0,), (0,)), ((), ())), preferred_element_type=jnp.float32
    )
    product = lax.dot_general(
        grad_low, whole_low, (((1,), (1,)), ((), ())), preferred_element_type=jnp.float32
    )
    outer = product
    left_sum, right_sum, outer = (left_sum, right_sum, outer)
    grad_square = jnp.sum(grad * grad)
    left_new = decay_rate * left_stat + (1.0 - decay_rate) * (outer / block)[None]
    right_new = decay_rate * right_stat + (1.0 - decay_rate) * (right_sum / width)[None]
    applied = left_sum.astype(jnp.bfloat16)
    update = jnp.dot(applied, right_root[0], preferred_element_type=jnp.float32)
    update_square = jnp.sum(update * update)
    total_grad, total_update = (by_axis(grad_square, FS_TP), by_axis(update_square, FS_TP))
    scale = jnp.sqrt(total_grad + 1.0) / jnp.sqrt(total_update + 1.0)
    step = scale * update
    new_weight = weight - step_size * step
    weight_copy = gathered_by_axis(new_weight.astype(jnp.bfloat16), FS, (0, 1, 2), 0)
    return (new_weight, step, left_new, right_new, weight_copy)


def solution(mesh):
    torus = Mesh(mesh.devices.reshape(8, 8, 2, mesh.shape["tp"]), ("fs_0", "fs_1", "fs_2", "tp"))
    return jax.shard_map(
        body,
        mesh=torus,
        in_specs=(
            P(FS, "tp"),
            P(FS, "tp"),
            P(FS, "tp"),
            P("tp", FS, None),
            P("tp", None, None),
            P("tp", FS, None),
            P("tp", FS, None),
        ),
        out_specs=(P(FS, "tp"), P(FS, "tp"), P("tp", FS, None), P("tp", FS, None), P(None, "tp")),
        check_vma=False,
    )
```

profile of v0, /device:TPU:1, one launch (start us, length us, event | category | flops | bytes accessed | tf_op | source)
XLA Modules:
  0.0 400.5 jit_solution(8813950215224952123)
XLA Ops:
  7.2 0.0 all-gather.4.cloned.1.call-start
  7.2 0.7 all-gather.4.cloned.1.call-update
  7.9 0.0 all-reduce.6.cloned.1.call-start
  8.0 52.3 %all-gather.4.cloned.1.call-done = bf16[768,2048]{1,0:T(8,128)(2,1)} async-done(((bf16[768,512]{1,0:T(8,128)(2,1)}), bf16[768,2048]{1,0:T(8,128)(2,1)}) %all-gather.4.cloned.1.call-update) | async-done | bytes 3145744 | tf_op jit(solution)/shard_map/all_gather | solution.py:47
  60.2 5.4 %fusion.14 = f32[2048,384]{1,0:T(8,128)} fusion(bf16[768,2048]{1,0:T(8,128)(2,1)} %all-gather.4.cloned.1.call-done, bf16[768,384]{1,0:T(8,128)(2,1)S(1)} %copy-done), kind=kOutput, calls=%fused_computation.20 | convolution fusion | flops 1207959552 | bytes 6881280 | tf_op jit(solution)/shard_map/dot_general | solution.py:49
  65.7 0.0 all-reduce.6.cloned.1.call-update
  65.7 0.0 all-gather.6.cloned.1.call-start
  65.8 203.9 %all-reduce.6.cloned.1.call-done = f32[2048,384]{1,0:T(8,128)} async-done(((f32[2048,384]{1,0:T(8,128)}), f32[2048,384]{1,0:T(8,128)}) %all-reduce.6.cloned.1.call-update) | async-done | bytes 3145744 | tf_op jit(solution)/shard_map/psum | solution.py:48
  269.7 2.1 convert_element_type.13
  271.8 1.4 multiply_reduce_fusion
  273.2 1.3 multiply_reduce_fusion.1
  274.6 13.3 %all-reduce.1 = (f32[]{:T(128)}, f32[]{:T(128)}) all-reduce(f32[]{:T(128)} %multiply_reduce_fusion.1, f32[]{:T(128)} %get-tuple-element.26), channel_id=1, replica_groups=mesh['fs_0'=8,'fs_1'=8,'fs_2'=2,'tp'=4] {'fs_0'}, use_global_device_ids=true, to_apply=%region_2.0 | all-reduce | flops 2 | bytes 16 | tf_op jit(solution)/shard_map/psum | solution.py:17
  287.8 14.7 %all-reduce = (f32[]{:T(128)}, f32[]{:T(128)}) all-reduce(f32[]{:T(128)} %get-tuple-element.17, f32[]{:T(128)} %get-tuple-element.18), channel_id=1, replica_groups=mesh['fs_0'=8,'fs_1'=8,'fs_2'=2,'tp'=4] {'fs_1'}, use_global_device_ids=true, to_apply=%region_3.0 | all-reduce | flops 2 | bytes 16 | tf_op jit(solution)/shard_map/psum | solution.py:17
  302.6 9.2 %all-reduce.3 = (f32[]{:T(128)}, f32[]{:T(128)}) all-reduce(f32[]{:T(128)} %get-tuple-element.15, f32[]{:T(128)} %get-tuple-element.16), channel_id=1, replica_groups=mesh['fs_0'=8,'fs_1'=8,'fs_2'=2,'tp'=4] {'fs_2'}, use_global_device_ids=true, to_apply=%region_4.0 | all-reduce | flops 2 | bytes 16 | tf_op jit(solution)/shard_map/psum | solution.py:17
  311.8 9.0 %all-reduce.2 = (f32[]{:T(128)}, f32[]{:T(128)}) all-reduce(f32[]{:T(128)} %get-tuple-element.21, f32[]{:T(128)} %get-tuple-element.22), channel_id=1, replica_groups=mesh['fs_0'=8,'fs_1'=8,'fs_2'=2,'tp'=4] {'tp'}, use_global_device_ids=true, to_apply=%region_5.0 | all-reduce | flops 2 | bytes 16 | tf_op jit(solution)/shard_map/psum | solution.py:17
  322.2 0.6 fusion.11
  322.8 18.5 %all-gather = bf16[128,384]{1,0:T(8,128)(2,1)S(1)} all-gather(bf16[16,384]{1,0:T(8,128)(2,1)S(1)} %get-tuple-element.23), channel_id=2, replica_groups=mesh['fs_0'=8,'fs_1'=8,'fs_2'=2,'tp'=4] {'fs_0'}, dimensions={0}, use_global_device_ids=true | all-gather | bytes 110592 | tf_op jit(solution)/shard_map/all_gather | solution.py:30
  341.3 22.1 %all_gather.14 = bf16[64,16,384]{2,1,0:T(8,128)(2,1)} all-gather(bf16[8,16,384]{2,1,0:T(8,128)(2,1)S(1)} %bitcast.31), channel_id=1, replica_groups=mesh['fs_0'=8,'fs_1'=8,'fs_2'=2,'tp'=4] {'fs_1'}, dimensions={0}, use_global_device_ids=true | all-gather | bytes 884736 | tf_op jit(solution)/shard_map/all_gather | solution.py:30
  363.4 0.0 all-gather.6.cloned.1.call-update
  363.5 0.6 fusion.4
  364.1 0.6 copy.17
  364.7 1.9 fusion.1
  366.6 24.6 %all-gather.6.cloned.1.call-done = bf16[128,16,384]{2,1,0:T(8,128)(2,1)} async-done(((bf16[64,16,384]{2,1,0:T(8,128)(2,1)}), bf16[128,16,384]{2,1,0:T(8,128)(2,1)}) %all-gather.6.cloned.1.call-update) | async-done | bytes 1572880 | tf_op jit(solution)/shard_map/all_gather | solution.py:30
  391.3 2.7 copy.16
  (12 shorter events, 0.0 us)
Async XLA Ops:
  7.2 53.1 %copy-start = (bf16[768,384]{1,0:T(8,128)(2,1)S(1)}, bf16[768,384]{1,0:T(8,128)(2,1)}, u32[]{:S(2)}) copy-start(bf16[768,384]{1,0:T(8,128)(2,1)} %param.7) | copy-start | bytes 1769476
  7.2 53.1 %all-gather.4.cloned.1.call-start = ((), (), s32[]{:S(2)}) async-start(), calls=%async_computation | async-start | bytes 3932160 | tf_op jit(solution)/shard_map/all_gather | solution.py:47
  7.9 261.8 %all-reduce.6.cloned.1.call-start = ((), (), s32[]{:S(2)}) async-start(), calls=%async_computation.1 | async-start | bytes 6291456 | tf_op jit(solution)/shard_map/psum | solution.py:48
  65.7 325.6 %all-gather.6.cloned.1.call-start = ((), (), s32[]{:S(2)}) async-start(), calls=%async_computation.2 | async-start | bytes 2359296 | tf_op jit(solution)/shard_map/all_gather | solution.py:30
  65.8 206.0 %copy-start.4 = (bf16[1,384,384]{2,1,0:T(8,128)(2,1)S(1)}, bf16[1,384,384]{2,1,0:T(8,128)(2,1)}, u32[]{:S(2)}) copy-start(bf16[1,384,384]{2,1,0:T(8,128)(2,1)} %param.11) | copy-start | bytes 884740
  65.8 206.0 %copy-start.5 = (bf16[1,16,2048]{2,1,0:T(8,128)(2,1)S(1)}, bf16[1,16,2048]{2,1,0:T(8,128)(2,1)}, u32[]{:S(2)}) copy-start(bf16[1,16,2048]{2,1,0:T(8,128)(2,1)} %param.10) | copy-start | bytes 196612
  271.8 50.4 %copy-start.2 = (f32[16,384]{1,0:T(8,128)S(1)}, f32[16,384]{1,0:T(8,128)}, u32[]{:S(2)}) copy-start(f32[16,384]{1,0:T(8,128)} %param.9) | copy-start | bytes 73732
  271.8 91.7 %copy-start.3 = (f32[1,3,384]{2,0,1:T(1,128)S(1)}, f32[1,3,384]{2,0,1:T(1,128)}, u32[]{:S(2)}) copy-start(f32[1,3,384]{2,0,1:T(1,128)} %param.13) | copy-start | bytes 13828
  341.3 23.4 %copy-start.1 = (f32[1,16,2048]{2,1,0:T(8,128)S(1)}, f32[1,16,2048]{2,1,0:T(8,128)}, u32[]{:S(2)}) copy-start(f32[1,16,2048]{2,1,0:T(8,128)} %param.12) | copy-start | bytes 393220
Sparse Core Ops, SparseCore 0:
  10.1 50.1 all-gather.3
  65.8 203.8 all-reduce.5
  363.6 27.6 all-gather.5
where the time goes:
time: 401 us
  waiting for transfers between devices  282 us (70%)
  blocking collectives  86.9 us (22%)
  between operations  15.2 us (4%)
  matrix products  9.37 us (2%)
  other arithmetic  4.03 us (1%)
    psum x1, waiting for transfers between devices, body(): lax.psum(lax.dot_general(cotangent, rnn_out, (((0,), (0,)), ((), ())), pr...  204 us
    all_gather x1, waiting for transfers between devices, body(): cotangent = lax.all_gather(out_grad, 'tp', axis=1, tiled=True)  52.3 us
    psum x4, blocking collectives, by_axis(): shard = lax.psum(shard, axis)  46.2 us
    all_gather x2, blocking collectives, stacked_from(): pieces = lax.all_gather(pieces, axes[k], axis=0, tiled=True)  40.7 us
    all_gather x1, waiting for transfers between devices, stacked_from(): pieces = lax.all_gather(pieces, axes[k], axis=0, tiled=True)  24.6 us
  transfers between devices with their start and end apart: 3, of which 3 were waited for; matrix products, arithmetic and copies ran while one was open for 1% of the time, Pallas kernels for 0%

commit v1 on v0

v1 whole, which is shorter than its diff:
```python
import functools

import jax
import jax.numpy as jnp
from jax import lax
from jax.experimental import pallas as pl
from jax.experimental.pallas import tpu as pltpu
from jax.sharding import Mesh
from jax.sharding import PartitionSpec as P

FS = ("fs_0", "fs_1", "fs_2")
MESH = pl.DeviceIdType.MESH
N = 8
F32 = jnp.float32
BF16 = jnp.bfloat16

decay_rate = 0.8
step_size = 0.005


def kernel(
    rnn_hbm, cot_hbm, w_hbm, lroot_hbm, rroot_hbm, lstat_hbm, rstat_hbm,
    nw_hbm, step_hbm, left_hbm, right_hbm, wc_hbm,
    rnn_own, rnn_in, cot_own, cot_in, w_v, lroot, rroot, lstat, rstat,
    part, part_in, rs1_out, rs1_in, rs2_out, rs2_in, G, A, W, upd, sc_own, sc_in,
    nw_v, step_v, left_v, right_v, wc_v,
    load_sem, store_sem,
    x_s, x_r, d2d_s, d2d_r, rs1_s, rs1_r, rs2_s, rs2_r,
    p1_s, p1_r, p2_s, p2_r, fw_s, fw_r, sc_s, sc_r,
):
    z, y, c, x = (lax.axis_index(a) for a in ("fs_0", "fs_1", "fs_2", "tp"))
    rem = lax.rem
    o = y + c * (z - y)
    i = z + c * (y - z)
    x_rnn = x + 1 - 2 * rem(x, 2)
    x_cot = 3 - x
    q_me, h_me = i // 2, rem(i, 2)
    odd_me = rem(q_me, 2)
    high = rem(x // 2 + q_me // 2, 2)
    low = rem(rem(x, 2) + rem((q_me + 1) // 2, 2), 2)
    blk_me = 2 * high + low

    def outer(k):
        return (rem(z + c * k, N), rem(y + (1 - c) * k, N), c, x)

    def inner(k):
        return (rem(z + (1 - c) * k, N), rem(y + c * k, N), c, x)

    def inner_at(j, xx):
        return (z + (1 - c) * (j - z), y + c * (j - y), c, xx)

    partner = (z, y, 1 - c, x)

    def remote(src, dst, s, r, to):
        return pltpu.make_async_remote_copy(
            src_ref=src, dst_ref=dst, send_sem=s, recv_sem=r, device_id=to, device_id_type=MESH
        )

    def settle(ref, sem):
        pltpu.make_async_copy(ref, ref, sem).wait()

    loads = [
        pltpu.make_async_copy(src, dst, load_sem.at[n])
        for n, (src, dst) in enumerate(
            [(cot_hbm, cot_own), (rnn_hbm, rnn_own), (w_hbm, w_v), (rroot_hbm, rroot), (lroot_hbm, lroot),
             (lstat_hbm, lstat), (rstat_hbm, rstat)]
        )
    ]
    for load in loads:
        load.start()

    barrier = pltpu.get_barrier_semaphore()

    def greet(k, _):
        pl.semaphore_signal(barrier, inc=1, device_id=outer(k), device_id_type=MESH)
        pl.semaphore_signal(barrier, inc=1, device_id=inner(k), device_id_type=MESH)
        zi, yi, _, _ = inner(k)
        pl.semaphore_signal(barrier, inc=1, device_id=(zi, yi, c, x_rnn), device_id_type=MESH)
        return 0

    lax.fori_loop(1, N, greet, 0)
    for k in range(1, 4):
        pl.semaphore_signal(barrier, inc=1, device_id=(z, y, c, rem(x + k, 4)), device_id_type=MESH)
    pl.semaphore_signal(barrier, inc=1, device_id=partner, device_id_type=MESH)
    pl.semaphore_wait(barrier, 3 * (N - 1) + 4)

    x_copies = []
    loads[0].wait()
    for h in range(2):
        cols = pl.ds(256 * h, 256)
        x_copies.append(remote(cot_own.at[:, cols], cot_in.at[h], x_s.at[h], x_r.at[h], (z, y, c, x_cot)))
    loads[1].wait()
    x_copies.append(remote(rnn_own, rnn_in, x_s.at[2], x_r.at[2], (z, y, c, x_rnn)))
    for n in (0, 2, 1):
        x_copies[n].start()

    def gather_1(t, mine):
        def send(k, _):
            remote(mine, mine, p1_s.at[t], p1_r.at[t], inner(k)).start()
            return 0

        lax.fori_loop(1, N, send, 0)

    def gather_2(t, block, both):
        settle(both.at[pl.ds(0, N - 1)], p1_r.at[t])
        settle(both.at[pl.ds(0, N - 1)], p1_s.at[t])

        def send(k, _):
            remote(block, block, p2_s.at[t, k], p2_r.at[t, k], outer(rem(k + 3, N - 1) + 1)).start()
            return 0

        lax.fori_loop(0, N - 1, send, 0)
        remote(block, block, fw_s.at[t], fw_r.at[t], partner).start()

    def gather_3(t, at, sized):
        def forward(k, _):
            off = rem(k + 3, N - 1) + 1
            src = rem(o - off + N, N)
            settle(at(src), p2_r.at[t, k])
            remote(at(src), at(src), fw_s.at[t], fw_r.at[t], partner).start()
            return 0

        lax.fori_loop(0, N - 1, forward, 0)

    def gather_4(t, at, sized):
        settle(sized, fw_r.at[t])
        settle(sized, fw_s.at[t])

        def sent(k, _):
            settle(at(o), p2_s.at[t, k])
            return 0

        lax.fori_loop(0, N - 1, sent, 0)

    loads[2].wait()
    W[c, o, i] = w_v[...].astype(BF16)
    gather_1(0, W.at[c, o, i])

    def product(cot, rnn):
        return lax.dot_general(cot, rnn, (((0,), (0,)), ((), ())), preferred_element_type=F32)

    def d2d(j):
        return remote(part.at[j, 1 - c], part_in.at[j], d2d_s.at[j], d2d_r.at[j], partner)

    def compute(j):
        q, h = j // 2, j % 2
        cot = cot_own[:, 256 * h:256 * h + 256] if q < 2 else cot_in[h]
        rnn = rnn_own[...] if q % 2 == 0 else rnn_in[...]
        part[j] = product(cot, rnn).reshape(2, N, 16, 384)
        d2d(j).start()

    def scatter_1(j):
        d2d(j).wait_recv()
        both = part[j, c] + part_in[j]
        part_in[j] = both
        rs1_out[j] = both.astype(BF16)

        def send(k, _):
            remote(rs1_out.at[j, rem(o + k, N)], rs1_in.at[j, k - 1], rs1_s.at[j], rs1_r.at[j], outer(k)).start()
            return 0

        lax.fori_loop(1, N, send, 0)

    def scatter_2(j):
        settle(rs1_in.at[j], rs1_r.at[j])
        total = part_in[j, o]
        for k in range(N - 1):
            total = total + rs1_in[j, k].astype(F32)
        rs2_out[j] = total
        odd = (j // 2) % 2 == 1
        if odd:
            remote(rs2_out.at[j], rs2_in.at[i], rs2_s.at[j], rs2_r.at[i], inner_at(j, x_rnn)).start()
        else:
            @pl.when(i != j)
            def _():
                remote(rs2_out.at[j], rs2_in.at[i], rs2_s.at[j], rs2_r.at[i], inner_at(j, x)).start()

            @pl.when(i == j)
            def _():
                rs2_in[i] = total

    compute(0)
    compute(1)
    scatter_1(0)
    scatter_1(1)
    gather_2(0, W.at[c, o], W.at[c, o])
    x_copies[0].wait_recv()
    compute(4)
    scatter_2(0)
    scatter_2(1)
    scatter_1(4)
    gather_3(0, lambda s: W.at[c, s], None)
    x_copies[2].wait_recv()
    compute(2)
    compute(3)
    compute(6)
    scatter_1(2)
    scatter_1(3)
    scatter_1(6)
    scatter_2(4)
    x_copies[1].wait_recv()
    compute(5)
    compute(7)
    scatter_2(2)
    scatter_2(3)
    scatter_2(6)
    scatter_1(5)
    scatter_1(7)
    scatter_2(5)
    scatter_2(7)

    def arrived(s, _):
        @pl.when((odd_me == 1) | (s != i))
        def _():
            settle(rs2_in.at[s], rs2_r.at[s])

        return 0

    lax.fori_loop(0, N, arrived, 0)
    piece = rs2_in[0]
    for s in range(1, N):
        piece = piece + rs2_in[s]
    G[blk_me, h_me, c, o] = piece.astype(BF16)
    gather_1(1, G.at[blk_me, h_me, c, o])
    loads[3].wait()
    loads[4].wait()
    loads[5].wait()
    loads[6].wait()
    gather_2(1, G.at[:, :, c, o], W.at[c, o])
    gather_3(1, lambda s: G.at[:, :, c, s], None)
    gather_4(1, lambda s: G.at[:, :, c, s], G.at[:, :, 1 - c])

    grad = G[...].reshape(2048, 384)
    rows = jnp.dot(lroot[...], grad, preferred_element_type=F32)
    A[c, o, i] = rows.astype(BF16)
    gather_1(2, A.at[c, o, i])

    gsq = jnp.zeros((128, 384), F32)
    for b in range(4):
        for h in range(2):
            for s in range(2):
                block = G[b, h, s].reshape(128, 384).astype(F32)
                gsq = gsq + block * block
    gather_2(2, A.at[c, o], A.at[c, o])

    index = (z * N + y) * 2 + c
    own = G[z // 2, rem(z, 2), y // 4, rem(y, 4) * 2 + c]
    outer_sum = lax.dot_general(own, grad, (((1,), (1,)), ((), ())), preferred_element_type=F32)
    left_v[...] = decay_rate * lstat[...] + (1.0 - decay_rate) * (outer_sum / 384)
    pick_row = lax.broadcasted_iota(jnp.int32, (16, 384), 0)
    pick_col = lax.broadcasted_iota(jnp.int32, (16, 384), 1)
    pick = jnp.where((pick_col == 3 * index + pick_row) & (pick_row < 3), 1.0, 0.0).astype(BF16)
    columns = lax.dot_general(pick, grad, (((1,), (1,)), ((), ())), preferred_element_type=F32).astype(BF16)
    right_sum = jnp.dot(columns, grad, preferred_element_type=F32)
    right_v[...] = decay_rate * rstat[...] + (1.0 - decay_rate) * (right_sum[0:3] / 2048)
    stores = [
        pltpu.make_async_copy(left_v, left_hbm, store_sem.at[0]),
        pltpu.make_async_copy(right_v, right_hbm, store_sem.at[1]),
    ]
    for store in stores:
        store.start()

    gather_3(2, lambda s: A.at[c, s], None)
    gather_4(2, lambda s: A.at[c, s], A.at[1 - c])

    usq = jnp.zeros((128, 384), F32)
    for cc in range(2):
        for oo in range(N):
            value = jnp.dot(A[cc, oo].reshape(128, 384), rroot[...], preferred_element_type=F32)
            upd[cc, oo] = value.reshape(N, 16, 384)
            usq = usq + value * value
    line = lax.broadcasted_iota(jnp.int32, (8, 128), 0)
    sc_own[...] = jnp.where(line == 0, jnp.sum(gsq), jnp.sum(usq))
    for k in range(1, 4):
        remote(sc_own, sc_in.at[k - 1], sc_s.at[k - 1], sc_r.at[k - 1], (z, y, c, rem(x + k, 4))).start()

    gather_4(0, lambda s: W.at[c, s], W.at[1 - c])

    for k in range(3):
        settle(sc_own, sc_r.at[k])
    sums = sc_own[...] + sc_in[0] + sc_in[1] + sc_in[2]
    scale = jnp.sqrt(sums[0:1, 0:1] + 1.0) / jnp.sqrt(sums[1:2, 0:1] + 1.0)
    step = scale * upd[c, o, i]
    step_v[...] = step
    nw_v[...] = w_v[...] - step_size * step
    stores.append(pltpu.make_async_copy(step_v, step_hbm, store_sem.at[2]))
    stores.append(pltpu.make_async_copy(nw_v, nw_hbm, store_sem.at[3]))
    stores[2].start()
    stores[3].start()
    for oo in range(N):
        for ii in range(N):
            first = W[0, oo, ii].astype(F32) - step_size * (scale * upd[0, oo, ii])
            wc_v[ii, oo, 0] = first.astype(BF16)
            second = W[1, oo, ii].astype(F32) - step_size * (scale * upd[1, oo, ii])
            wc_v[oo, ii, 1] = second.astype(BF16)
    stores.append(pltpu.make_async_copy(wc_v, wc_hbm, store_sem.at[4]))
    stores[4].start()

    for n in range(3):
        x_copies[n].wait_send()
        settle(sc_own, sc_s.at[n])
    for j in range(N):
        d2d(j).wait_send()
        settle(rs1_in.at[j], rs1_s.at[j])
        if (j // 2) % 2 == 1:
            settle(rs2_out.at[j], rs2_s.at[j])
        else:
            @pl.when(i != j)
            def _():
                settle(rs2_out.at[j], rs2_s.at[j])

    for store in stores:
        store.wait()


def body(rnn_out, out_grad, weight, left_root, right_root, left_stat, right_stat):
    tokens = rnn_out.shape[0]
    hbm = pl.BlockSpec(memory_space=pl.ANY)
    v = pltpu.VMEM
    dma = pltpu.SemaphoreType.DMA
    outs = pl.pallas_call(
        kernel,
        name="step",
        out_shape=(
            jax.ShapeDtypeStruct((16, 384), F32),
            jax.ShapeDtypeStruct((16, 384), F32),
            jax.ShapeDtypeStruct((16, 2048), F32),
            jax.ShapeDtypeStruct((3, 384), F32),
            jax.ShapeDtypeStruct((N, N, 2, 16, 384), BF16),
        ),
        in_specs=[hbm] * 7,
        out_specs=(hbm,) * 5,
        scratch_shapes=[
            v((tokens, 384), BF16), v((tokens, 384), BF16), v((tokens, 512), BF16), v((2, tokens, 256), BF16),
            v((16, 384), F32), v((16, 2048), BF16), v((384, 384), BF16), v((16, 2048), F32), v((3, 384), F32),
            v((N, 2, N, 16, 384), F32), v((N, N, 16, 384), F32),
            v((N, N, 16, 384), BF16), v((N, N - 1, 16, 384), BF16),
            v((N, 16, 384), F32), v((N, 16, 384), F32),
            v((4, 2, 2, N, 16, 384), BF16), v((2, N, N, 16, 384), BF16), v((2, N, N, 16, 384), BF16),
            v((2, N, N, 16, 384), F32), v((8, 128), F32), v((3, 8, 128), F32),
            v((16, 384), F32), v((16, 384), F32), v((16, 2048), F32), v((3, 384), F32), v((N, N, 2, 16, 384), BF16),
            dma((7,)), dma((5,)),
            dma((3,)), dma((3,)), dma((N,)), dma((N,)), dma((N,)), dma((N,)), dma((N,)), dma((N,)),
            dma((3,)), dma((3,)), dma((3, N - 1)), dma((3, N - 1)), dma((3,)), dma((3,)), dma((3,)), dma((3,)),
        ],
        compiler_params=pltpu.CompilerParams(collective_id=0, has_side_effects=True),
    )(rnn_out, out_grad, weight, left_root[0], right_root[0], left_stat[0], right_stat[0])
    new_weight, step, left_new, right_new, copy = outs
    return new_weight, step, left_new[None], right_new[None], copy.reshape(2048, 384)


def solution(mesh):
    torus = Mesh(mesh.devices.reshape(N, N, 2, mesh.shape["tp"]), ("fs_0", "fs_1", "fs_2", "tp"))
    return jax.shard_map(
        body,
        mesh=torus,
        in_specs=(
            P(FS, "tp"),
            P(FS, "tp"),
            P(FS, "tp"),
            P("tp", FS, None),
            P("tp", None, None),
            P("tp", FS, None),
            P("tp", FS, None),
        ),
        out_specs=(P(FS, "tp"), P(FS, "tp"), P("tp", FS, None), P("tp", FS, None), P(None, "tp")),
        check_vma=False,
    )
```

time: 401 us -> 107 us (0.27)
  waiting for transfers between devices: 282 us -> 0 us
  Pallas kernels: 0 us -> 96.7 us
  blocking collectives: 86.9 us -> 0 us
  between operations: 15.2 us -> 0.64 us
  matrix products: 9.37 us -> 0 us
  local copies, waits for them, and re-layouts: 3.4 us -> 9.54 us
  other arithmetic: 4.03 us -> 0 us
    psum x1 -> x0, waiting for transfers between devices: 204 us -> none  [body(): lax.psum(lax.dot_general(cotangent, rnn_out, (((0,), (0,)), ((), ())), pr...]
    pallas_call x0 -> x1, Pallas kernels: none -> 96.7 us  [body(): pl.pallas_call(kernel, name='step', out_shape=(jax.ShapeDtypeStruct((16,...]
    all_gather x2 -> x0, waiting for transfers between devices: 76.9 us -> none  [the longest x1 52.3 us: body(): cotangent = lax.all_gather(out_grad, 'tp', axis=1, tiled=True)]
    psum x4 -> x0, blocking collectives: 46.2 us -> none  [by_axis(): shard = lax.psum(shard, axis)]
    all_gather x2 -> x0, blocking collectives: 40.7 us -> none  [stacked_from(): pieces = lax.all_gather(pieces, axes[k], axis=0, tiled=True)]
    dot_general x4 -> x0, matrix products: 9.37 us -> none  [the longest x1 5.43 us: body(): lax.dot_general(cotangent, rnn_out, (((0,), (0,)), ((), ())), preferred_e...]
    unnamed x13 -> x6, local copies, waits for them, and re-layouts: 0.65 us -> 9.54 us
  transfers between devices with their start and end apart: 3 -> 0, of which waited for: 3 -> 0; matrix products, arithmetic and copies ran while one was open for 1% -> 0% of each run, Pallas kernels for 0% -> 0%
where the time goes in v1:
time: 107 us
  Pallas kernels  96.7 us (90%)
  local copies, waits for them, and re-layouts  9.54 us (9%)
    pallas_call x1, Pallas kernels, body(): pl.pallas_call(kernel, name='step', out_shape=(jax.ShapeDtypeStruct((16,...  96.7 us
    unnamed x6, local copies, waits for them, and re-layouts  9.54 us

profile of v1, /device:TPU:1, one launch (start us, length us, event | category | flops | bytes accessed | tf_op | source)
XLA Modules:
  0.0 106.9 jit_solution(11366773757548409438)
XLA Ops:
  0.6 1.3 %copy.15 = f32[1,3,384]{2,1,0:T(4,128)} copy(f32[1,3,384]{2,0,1:T(1,128)} %param.13) | data formatting | bytes 9216
  1.9 96.7 %step.1 = (f32[16,384]{1,0:T(8,128)}, f32[16,384]{1,0:T(8,128)}, f32[16,2048]{1,0:T(8,128)}, f32[3,384]{1,0:T(4,128)}, bf16[8,8,2,16,384]{4,3,2,1,0:T(8,128)(2,1)}) custom-call(bf16[768,384]{1,0:T(8,128)(2,1)} %rnn_hbm.1, bf16[768,512]{1,0:T(8,128)(2,1)} %cot_hbm.1, f32[16,384]{1,0:T(8,128)} %w_hbm.1, bf16[16,2048]{1,0:T(8,128)(2,1)} %bitcast.13, ...), custom_call_target="tpu_custom_call" | custom-call | tf_op jit(solution)/shard_map/step/pallas_call | solution.py:321
  98.6 1.3 %copy.12 = f32[1,3,384]{2,0,1:T(1,128)} copy(f32[1,3,384]{2,1,0:T(4,128)} %bitcast.15) | data formatting | bytes 9216
  99.9 1.3 %copy.20 = f32[16,384]{1,0:T(8,128)} copy(f32[16,384]{1,0:T(8,128)} %get-tuple-element.25) | data formatting | bytes 49152
  101.2 1.3 %copy.21 = f32[16,384]{1,0:T(8,128)} copy(f32[16,384]{1,0:T(8,128)} %get-tuple-element.26) | data formatting | bytes 49152
  102.6 1.6 %copy.22 = f32[1,16,2048]{2,1,0:T(8,128)} copy(f32[1,16,2048]{2,1,0:T(8,128)} %bitcast.12) | data formatting | bytes 262144
  104.2 2.7 %copy.23 = bf16[2048,384]{1,0:T(8,128)(2,1)} copy(bf16[2048,384]{1,0:T(8,128)(2,1)} %bitcast.9) | data formatting | bytes 3145728

commit v2 on v1

v2 whole, which is shorter than its diff:
```python
import functools

import jax
import jax.numpy as jnp
from jax import lax
from jax.experimental import pallas as pl
from jax.experimental.pallas import tpu as pltpu
from jax.sharding import Mesh
from jax.sharding import PartitionSpec as P

FS = ("fs_0", "fs_1", "fs_2")
MESH = pl.DeviceIdType.MESH
N = 8
F32 = jnp.float32
BF16 = jnp.bfloat16

decay_rate = 0.8
step_size = 0.005


def kernel(
    rnn_hbm, cot_hbm, w_hbm, lroot_hbm, rroot_hbm, lstat_hbm, rstat_hbm,
    nw_v, step_v, left_v, right_v, wc_v,
    rnn_own, rnn_in, cot_own, cot_in, w_v, lroot, rroot, lstat, rstat,
    part, part_in, rs1_out, rs1_in, ar_out, ar_in, G, A, W, upd, own_update, piece_v, t1, t2, t3, t3_in, t4,
    load_sem,
    x_s, x_r, d2d_s, d2d_r, rs1_s, rs1_r, ar_s, ar_r,
    g2_s, g2_r, g3_s, g3_r, a1_s, a1_r, a2_s, a2_r, a3_s, a3_r,
    w1_s, w1_r, w2_s, w2_r, w3_s, w3_r, t_s, t_r,
):
    z, y, c, x = (lax.axis_index(a) for a in ("fs_0", "fs_1", "fs_2", "tp"))
    rem = lax.rem
    o = y + c * (z - y)
    i = z + c * (y - z)
    x_rnn = x + 1 - 2 * rem(x, 2)
    x_cot = 3 - x
    blocks = (x, x_rnn, x_cot, rem(x + 2, 4))

    def outer(k):
        return (rem(z + c * k, N), rem(y + (1 - c) * k, N), c, x)

    def inner(k, xx=None):
        return (rem(z + (1 - c) * k, N), rem(y + c * k, N), c, x if xx is None else xx)

    def along_x(k):
        return (z, y, c, rem(x + k, 4))

    partner = (z, y, 1 - c, x)

    def remote(src, dst, s, r, to):
        return pltpu.make_async_remote_copy(
            src_ref=src, dst_ref=dst, send_sem=s, recv_sem=r, device_id=to, device_id_type=MESH
        )

    def settle(ref, sem):
        pltpu.make_async_copy(ref, ref, sem).wait()

    def to_all(ref, s, r, peers, count=N):
        def send(k, _):
            remote(ref, ref, s, r, peers(k)).start()
            return 0

        lax.fori_loop(1, count, send, 0)

    seven = rs1_in.at[0]

    loads = [
        pltpu.make_async_copy(src, dst, load_sem.at[n])
        for n, (src, dst) in enumerate(
            [(cot_hbm, cot_own), (rnn_hbm, rnn_own), (w_hbm, w_v), (rroot_hbm, rroot), (lroot_hbm, lroot),
             (lstat_hbm, lstat), (rstat_hbm, rstat)]
        )
    ]
    for load in loads:
        load.start()

    barrier = pltpu.get_barrier_semaphore()

    def greet(k, _):
        pl.semaphore_signal(barrier, inc=1, device_id=outer(k), device_id_type=MESH)
        pl.semaphore_signal(barrier, inc=1, device_id=inner(k), device_id_type=MESH)
        zi, yi, _, _ = inner(k)
        pl.semaphore_signal(barrier, inc=1, device_id=(zi, yi, c, x_rnn), device_id_type=MESH)
        return 0

    lax.fori_loop(1, N, greet, 0)
    for k in range(1, 4):
        pl.semaphore_signal(barrier, inc=1, device_id=along_x(k), device_id_type=MESH)
    pl.semaphore_signal(barrier, inc=1, device_id=partner, device_id_type=MESH)
    pl.semaphore_wait(barrier, 3 * (N - 1) + 4)

    x_copies = []
    loads[0].wait()
    for h in range(2):
        cols = pl.ds(256 * h, 256)
        x_copies.append(remote(cot_own.at[:, cols], cot_in.at[h], x_s.at[h], x_r.at[h], (z, y, c, x_cot)))
    loads[1].wait()
    x_copies.append(remote(rnn_own, rnn_in, x_s.at[2], x_r.at[2], (z, y, c, x_rnn)))
    for n in (0, 2, 1):
        x_copies[n].start()

    def weight_1():
        loads[2].wait()
        W[c, i, o] = w_v[...].astype(BF16)
        to_all(W.at[c, i, o], w1_s, w1_r, inner)

    def weight_2():
        settle(seven, w1_r)

        def send(k, _):
            row = W.at[c, :, o]
            remote(row, row, w2_s.at[k], w2_r.at[k], outer(rem(k + 3, N - 1) + 1)).start()
            return 0

        lax.fori_loop(0, N - 1, send, 0)

    def weight_3():
        def arrive(k, _):
            settle(W.at[c, :, o], w2_r.at[k])
            return 0

        lax.fori_loop(0, N - 1, arrive, 0)
        remote(W.at[c], W.at[c], w3_s, w3_r, partner).start()

    def product(cot, rnn):
        return lax.dot_general(cot, rnn, (((0,), (0,)), ((), ())), preferred_element_type=F32)

    def d2d(j):
        return remote(part.at[j, 1 - c], part_in.at[j], d2d_s.at[j], d2d_r.at[j], partner)

    def compute(j):
        q, h = j // 2, j % 2
        cot = cot_own[:, 256 * h:256 * h + 256] if q < 2 else cot_in[h]
        rnn = rnn_own[...] if q % 2 == 0 else rnn_in[...]
        part[j] = product(cot, rnn).reshape(2, N, 16, 384)
        d2d(j).start()

    def scatter_1(j):
        d2d(j).wait_recv()
        both = part[j, c] + part_in[j]
        part_in[j] = both
        rs1_out[j] = both.astype(BF16)

        def send(k, _):
            remote(rs1_out.at[j, rem(o + k, N)], rs1_in.at[j, k - 1], rs1_s.at[j], rs1_r.at[j], outer(k)).start()
            return 0

        lax.fori_loop(1, N, send, 0)

    def scatter_2(j):
        settle(seven, rs1_r.at[j])
        total = part_in[j, o]
        for k in range(N - 1):
            total = total + rs1_in[j, k].astype(F32)
        mine = total.astype(BF16)
        if (j // 2) % 2 == 1:
            ar_out[j] = mine

            def send(k, _):
                remote(ar_out.at[j], ar_in.at[j, i], ar_s.at[j], ar_r.at[j], inner(k, x_rnn)).start()
                return 0

            lax.fori_loop(0, N, send, 0)
        else:
            ar_in[j, i] = mine
            to_all(ar_in.at[j, i], ar_s.at[j], ar_r.at[j], inner)

    def g_piece(j):
        return G.at[blocks[j // 2], j % 2, c, o]

    def gather_2(j):
        settle(ar_in.at[j] if (j // 2) % 2 == 1 else seven, ar_r.at[j])
        piece = ar_in[j, 0].astype(F32)
        for s in range(1, N):
            piece = piece + ar_in[j, s].astype(F32)
        G[blocks[j // 2], j % 2, c, o] = piece.astype(BF16)

        @pl.when(i == j)
        def _():
            piece_v[...] = piece

        to_all(g_piece(j), g2_s.at[j], g2_r.at[j], outer)

    def gather_3(j):
        settle(seven, g2_r.at[j])
        both = G.at[blocks[j // 2], j % 2, c]
        remote(both, both, g3_s, g3_r, partner).start()

    weight_1()
    compute(0)
    compute(1)
    scatter_1(0)
    scatter_1(1)
    weight_2()
    x_copies[0].wait_recv()
    compute(4)
    scatter_2(0)
    scatter_2(1)
    scatter_1(4)
    x_copies[2].wait_recv()
    compute(2)
    compute(3)
    compute(6)
    scatter_1(2)
    scatter_1(3)
    scatter_1(6)
    gather_2(0)
    gather_2(1)
    scatter_2(4)
    x_copies[1].wait_recv()
    compute(5)
    compute(7)
    scatter_1(5)
    scatter_1(7)
    scatter_2(2)
    scatter_2(3)
    scatter_2(6)
    gather_2(4)
    scatter_2(5)
    scatter_2(7)
    gather_2(2)
    gather_2(3)
    gather_2(6)
    gather_3(0)
    gather_3(1)
    weight_3()
    gather_2(5)
    gather_2(7)
    gather_3(4)
    gather_3(2)
    gather_3(3)
    gather_3(6)
    gather_3(5)
    gather_3(7)
    for n in range(3, 7):
        loads[n].wait()
    settle(W.at[0], g3_r)

    grad = G[...].reshape(2048, 384)
    rows = jnp.dot(lroot[...], grad, preferred_element_type=F32).astype(BF16)
    A[c, i, o] = rows
    to_all(A.at[c, i, o], a1_s, a1_r.at[i], inner)

    update = jnp.dot(rows, rroot[...], preferred_element_type=F32)
    own_update[...] = update
    line = lax.broadcasted_iota(jnp.int32, (8, 128), 0)
    t1[o] = jnp.where(line == 0, jnp.sum(piece_v[...] * piece_v[...]), jnp.sum(update * update))
    to_all(t1.at[o], t_s.at[0], t_r.at[0], outer)
    to_all(A.at[c, i, o], a2_s.at[i], a2_r.at[i], outer)

    def relay(k, _):
        half = (k + 1) // 2
        j = rem(i + half + rem(k + 1, 2) * (N - 2 * half), N)
        settle(A.at[c, j, o], a1_r.at[j])
        to_all(A.at[c, j, o], a2_s.at[j], a2_r.at[j], outer)
        return 0

    lax.fori_loop(1, 5, relay, 0)

    def total_of(ref, count):
        total = ref[0]
        for s in range(1, count):
            total = total + ref[s]
        return total

    settle(t1.at[pl.ds(0, N - 1)], t_r.at[0])
    t2[i] = total_of(t1, N)
    to_all(t2.at[i], t_s.at[1], t_r.at[1], inner)
    lax.fori_loop(5, N, relay, 0)

    index = (z * N + y) * 2 + c
    own = G[z // 2, rem(z, 2), y // 4, rem(y, 4) * 2 + c]
    outer_sum = lax.dot_general(own, grad, (((1,), (1,)), ((), ())), preferred_element_type=F32)
    left_v[...] = decay_rate * lstat[...] + (1.0 - decay_rate) * (outer_sum / 384)
    pick_row = lax.broadcasted_iota(jnp.int32, (16, 384), 0)
    pick_col = lax.broadcasted_iota(jnp.int32, (16, 384), 1)
    pick = jnp.where((pick_col == 3 * index + pick_row) & (pick_row < 3), 1.0, 0.0).astype(BF16)
    columns = lax.dot_general(pick, grad, (((1,), (1,)), ((), ())), preferred_element_type=F32).astype(BF16)
    right_sum = jnp.dot(columns, grad, preferred_element_type=F32)
    for r in range(3):
        right_v[r] = decay_rate * rstat[r] + (1.0 - decay_rate) * (right_sum[r:r + 1] / 2048)

    settle(t2.at[pl.ds(0, N - 1)], t_r.at[1])
    t3[...] = total_of(t2, N)
    remote(t3, t3_in, t_s.at[2], t_r.at[2], partner).start()

    def pass_on(k):
        j = near(i, k)
        settle(seven, a2_r.at[j])
        remote(A.at[c, j], A.at[c, j], a3_s, a3_r.at[j], partner).start()
        multiply(c, j)

    def near(start, k):
        half = (k + 1) // 2
        return rem(start + half + ((k + 1) % 2) * (N - 2 * half), N)

    def multiply(core, j):
        upd[core, j] = jnp.dot(
            A[core, j].reshape(128, 384), rroot[...], preferred_element_type=F32
        ).reshape(N, 16, 384)

    def take(k):
        j = near(o, k)
        settle(A.at[c, j], a3_r.at[j])
        multiply(1 - c, j)

    pass_on(0)
    pass_on(1)
    pass_on(2)
    settle(t3, t_r.at[2])
    t4[x] = t3[...] + t3_in[...]
    to_all(t4.at[x], t_s.at[3], t_r.at[3], along_x, 4)
    pass_on(3)
    take(0)
    pass_on(4)
    take(1)
    take(2)
    pass_on(5)
    take(3)
    pass_on(6)
    take(4)
    pass_on(7)
    take(5)
    settle(W.at[1 - c], w3_r)
    settle(t4.at[pl.ds(0, 3)], t_r.at[3])
    sums = total_of(t4, 4)
    scale = jnp.sqrt(sums[0:1, 0:1] + 1.0) / jnp.sqrt(sums[1:2, 0:1] + 1.0)
    step = scale * own_update[...]
    step_v[...] = step
    nw_v[...] = w_v[...] - step_size * step
    take(6)
    take(7)
    for oo in range(N):
        for ii in range(N):
            first = W[0, ii, oo].astype(F32) - step_size * (scale * upd[0, ii, oo])
            wc_v[ii, oo, 0] = first.astype(BF16)
            second = W[1, ii, oo].astype(F32) - step_size * (scale * upd[1, ii, oo])
            wc_v[oo, ii, 1] = second.astype(BF16)

    for n in range(3):
        x_copies[n].wait_send()
    for j in range(N):
        d2d(j).wait_send()
        settle(seven, rs1_s.at[j])
        settle(seven, g2_s.at[j])
        settle(seven, a2_s.at[j])
        settle(ar_in.at[j] if (j // 2) % 2 == 1 else seven, ar_s.at[j])

    def sent(k, _):
        settle(W.at[c, :, o], w2_s.at[k])
        return 0

    lax.fori_loop(0, N - 1, sent, 0)
    settle(seven, a1_s)
    settle(seven, w1_s)
    for sem in (g3_s, a3_s, w3_s):
        settle(W.at[c], sem)
    settle(t1.at[pl.ds(0, N - 1)], t_s.at[0])
    settle(t2.at[pl.ds(0, N - 1)], t_s.at[1])
    settle(t3, t_s.at[2])
    settle(t4.at[pl.ds(0, 3)], t_s.at[3])


def write(*refs):
    *refs, sem = refs
    stores = [pltpu.make_async_copy(refs[n], refs[5 + n], sem.at[n]) for n in (4, 2, 0, 1, 3)]
    for store in stores:
        store.start()
    for store in stores:
        store.wait()


def body(rnn_out, out_grad, weight, left_root, right_root, left_stat, right_stat):
    tokens = rnn_out.shape[0]
    hbm = pl.BlockSpec(memory_space=pl.ANY)
    vmem = pl.BlockSpec(memory_space=pltpu.VMEM)
    v = pltpu.VMEM
    dma = pltpu.SemaphoreType.DMA
    outs = (((16, 384), F32), ((16, 384), F32), ((16, 2048), F32), ((3, 1, 384), F32), ((N, N, 2, 16, 384), BF16))
    results = pl.pallas_call(
        kernel,
        name="step",
        out_shape=tuple(pltpu.VMEM(*shape) for shape in outs),
        in_specs=[hbm] * 7,
        out_specs=(vmem,) * 5,
        scratch_shapes=[
            v((tokens, 384), BF16), v((tokens, 384), BF16), v((tokens, 512), BF16), v((2, tokens, 256), BF16),
            v((16, 384), F32), v((16, 2048), BF16), v((384, 384), BF16), v((16, 2048), F32), v((3, 1, 384), F32),
            v((N, 2, N, 16, 384), F32), v((N, N, 16, 384), F32),
            v((N, N, 16, 384), BF16), v((N, N - 1, 16, 384), BF16),
            v((N, 16, 384), BF16), v((N, N, 16, 384), BF16),
            v((4, 2, 2, N, 16, 384), BF16), v((2, N, N, 16, 384), BF16), v((2, N, N, 16, 384), BF16),
            v((2, N, N, 16, 384), F32), v((16, 384), F32), v((16, 384), F32),
            v((N, 8, 128), F32), v((N, 8, 128), F32), v((8, 128), F32), v((8, 128), F32), v((4, 8, 128), F32),
            dma((7,)),
            dma((3,)), dma((3,)), dma((N,)), dma((N,)), dma((N,)), dma((N,)), dma((N,)), dma((N,)),
            dma((N,)), dma((N,)), dma, dma, dma, dma((N,)), dma((N,)), dma((N,)), dma, dma((N,)),
            dma, dma, dma((N - 1,)), dma((N - 1,)), dma, dma, dma((4,)), dma((4,)),
        ],
        compiler_params=pltpu.CompilerParams(collective_id=0, has_side_effects=True),
    )(rnn_out, out_grad, weight, left_root[0], right_root[0], left_stat[0], jnp.transpose(right_stat, (1, 0, 2)))
    new_weight, step, left_new, right_new, copy = pl.pallas_call(
        write,
        name="write",
        out_shape=tuple(jax.ShapeDtypeStruct(*shape) for shape in outs),
        in_specs=[vmem] * 5,
        out_specs=(hbm,) * 5,
        scratch_shapes=[dma((5,))],
    )(*(pltpu.with_memory_space_constraint(result, pltpu.VMEM) for result in results))
    return new_weight, step, left_new[None], jnp.transpose(right_new, (1, 0, 2)), copy.reshape(2048, 384)


def solution(mesh):
    torus = Mesh(mesh.devices.reshape(N, N, 2, mesh.shape["tp"]), ("fs_0", "fs_1", "fs_2", "tp"))
    return jax.shard_map(
        body,
        mesh=torus,
        in_specs=(
            P(FS, "tp"),
            P(FS, "tp"),
            P(FS, "tp"),
            P("tp", FS, None),
            P("tp", None, None),
            P("tp", FS, None),
            P("tp", FS, None),
        ),
        out_specs=(P(FS, "tp"), P(FS, "tp"), P("tp", FS, None), P("tp", FS, None), P(None, "tp")),
        check_vma=False,
    )
```

time: 107 us -> 81.1 us (0.76)
  Pallas kernels: 96.7 us -> 80.3 us
  local copies, waits for them, and re-layouts: 9.54 us -> 0 us
    pallas_call x1 -> x2, Pallas kernels: 96.7 us -> 80.3 us  [the longest x1 79.1 us: body(): pl.pallas_call(kernel, name='step', out_shape=tuple((pltpu.VMEM(*shape) f...]
    unnamed x6 -> x0, local copies, waits for them, and re-layouts: 9.54 us -> none
where the time goes in v2:
time: 81.1 us; the launch traced here: 81 us
  Pallas kernels  80.3 us (99%)
    pallas_call x1, Pallas kernels, body(): pl.pallas_call(kernel, name='step', out_shape=tuple((pltpu.VMEM(*shape) f...  79.1 us

profile of v2, /device:TPU:1, one launch (start us, length us, event | category | flops | bytes accessed | tf_op | source)
XLA Modules:
  0.0 81.0 jit_solution(8214174597729837592)
XLA Ops:
  0.6 79.1 %step.1 = (f32[16,384]{1,0:T(8,128)S(1)}, f32[16,384]{1,0:T(8,128)S(1)}, f32[16,2048]{1,0:T(8,128)S(1)}, f32[3,1,384]{2,1,0:T(1,128)S(1)}, bf16[8,8,2,16,384]{4,3,2,1,0:T(8,128)(2,1)S(1)}) custom-call(bf16[768,384]{1,0:T(8,128)(2,1)} %rnn_hbm.1, bf16[768,512]{1,0:T(8,128)(2,1)} %cot_hbm.1, f32[16,384]{1,0:T(8,128)} %w_hbm.1, bf16[16,2048]{1,0:T(8,128)(2,1)} %bitcast.9, ...), custom_call_target="tpu_custom_call" | custom-call | tf_op jit(solution)/shard_map/step/pallas_call | solution.py:380
  79.7 1.2 %write.1 = (f32[16,384]{1,0:T(8,128)}, f32[16,384]{1,0:T(8,128)}, f32[16,2048]{1,0:T(8,128)}, f32[3,1,384]{2,1,0:T(1,128)}, bf16[8,8,2,16,384]{4,3,2,1,0:T(8,128)(2,1)}) custom-call(f32[16,384]{1,0:T(8,128)S(1)} %get-tuple-element.15.refs_0_, f32[16,384]{1,0:T(8,128)S(1)} %get-tuple-element.16.refs_1_, f32[16,2048]{1,0:T(8,128)S(1)} %get-tuple-element.17.refs_2_, ...), custom_call_target="tpu_custom_call" | custom-call | tf_op jit(solution)/shard_map/write/pallas_call | solution.py:402

commit v3 on v2

--- a/solution.py
+++ b/solution.py
@@ -18,14 +18,18 @@
 step_size = 0.005
 
 
+LAST = (5, 7)
+FAR_FIRST = (4, 5, 3, 6, 2, 7, 1)
+
+
 def kernel(
     rnn_hbm, cot_hbm, w_hbm, lroot_hbm, rroot_hbm, lstat_hbm, rstat_hbm,
     nw_v, step_v, left_v, right_v, wc_v,
     rnn_own, rnn_in, cot_own, cot_in, w_v, lroot, rroot, lstat, rstat,
-    part, part_in, rs1_out, rs1_in, ar_out, ar_in, G, A, W, upd, own_update, piece_v, t1, t2, t3, t3_in, t4,
-    load_sem,
+    part, part_in, rs1_out, rs1_in, ar_out, ar_in, G, A, W, upd, own_update, piece_v, t1, t2, t3,
+    load_sem, known,
     x_s, x_r, d2d_s, d2d_r, rs1_s, rs1_r, ar_s, ar_r,
-    g2_s, g2_r, g3_s, g3_r, a1_s, a1_r, a2_s, a2_r, a3_s, a3_r,
+    g2_s, g2_r, g2_up, g2_down, g3_s, g3_r, a1_s, a1_r, a2_s, a2_r, a2_up, a2_down, a3_s, a3_r,
     w1_s, w1_r, w2_s, w2_r, w3_s, w3_r, t_s, t_r,
 ):
     z, y, c, x = (lax.axis_index(a) for a in ("fs_0", "fs_1", "fs_2", "tp"))
@@ -42,8 +46,8 @@
     def inner(k, xx=None):
         return (rem(z + (1 - c) * k, N), rem(y + c * k, N), c, x if xx is None else xx)
 
-    def along_x(k):
-        return (z, y, c, rem(x + k, 4))
+    def chip_x(k):
+        return (z, y, rem(c + k // 4, 2), rem(x + k, 4))
 
     partner = (z, y, 1 - c, x)
 
@@ -55,14 +59,24 @@
     def settle(ref, sem):
         pltpu.make_async_copy(ref, ref, sem).wait()
 
-    def to_all(ref, s, r, peers, count=N):
-        def send(k, _):
+    def to_all(ref, s, r, peers, order=FAR_FIRST):
+        for k in order:
             remote(ref, ref, s, r, peers(k)).start()
-            return 0
-
-        lax.fori_loop(1, count, send, 0)
 
     seven = rs1_in.at[0]
+    five = rs1_in.at[0, pl.ds(0, 5)]
+    def spread(at, s, r, up, down):
+        for k, sem in ((2, up), (N - 2, down), (1, r(1)), (N - 1, r(N - 1))):
+            remote(at(o), at(o), s, sem, outer(k)).start()
+
+    def relay(at, s, r, up, down, four_up):
+        for away, sem in ((N - 2, up), (2, down)):
+            ref = at(rem(o + away, N))
+            settle(ref, sem)
+            turn = N - away
+            if four_up == (away == N - 2):
+                remote(ref, ref, s, r(4), outer(turn)).start()
+            remote(ref, ref, s, r(3 if turn == 2 else 5), outer(1 if turn == 2 else N - 1)).start()
 
     loads = [
         pltpu.make_async_copy(src, dst, load_sem.at[n])
@@ -75,19 +89,17 @@
         load.start()
 
     barrier = pltpu.get_barrier_semaphore()
-
-    def greet(k, _):
-        pl.semaphore_signal(barrier, inc=1, device_id=outer(k), device_id_type=MESH)
-        pl.semaphore_signal(barrier, inc=1, device_id=inner(k), device_id_type=MESH)
-        zi, yi, _, _ = inner(k)
-        pl.semaphore_signal(barrier, inc=1, device_id=(zi, yi, c, x_rnn), device_id_type=MESH)
-        return 0
-
-    lax.fori_loop(1, N, greet, 0)
-    for k in range(1, 4):
-        pl.semaphore_signal(barrier, inc=1, device_id=along_x(k), device_id_type=MESH)
-    pl.semaphore_signal(barrier, inc=1, device_id=partner, device_id_type=MESH)
-    pl.semaphore_wait(barrier, 3 * (N - 1) + 4)
+    near_by = (outer(1), outer(N - 1), inner(1), inner(N - 1))
+    for to in ((z, y, c, x_cot), (z, y, c, x_rnn), partner) + near_by:
+        pl.semaphore_signal(barrier, inc=1, device_id=to, device_id_type=MESH)
+    pl.semaphore_wait(barrier, 7)
+
+    def learn(n, devices):
+        for to in devices:
+            pl.semaphore_signal(known.at[n], inc=1, device_id=to, device_id_type=MESH)
+
+    def learned(n, count):
+        pl.semaphore_wait(known.at[n], count)
 
     x_copies = []
     loads[0].wait()
@@ -98,28 +110,31 @@
     x_copies.append(remote(rnn_own, rnn_in, x_s.at[2], x_r.at[2], (z, y, c, x_rnn)))
     for n in (0, 2, 1):
         x_copies[n].start()
+    learn(0, near_by)
 
     def weight_1():
         loads[2].wait()
         W[c, i, o] = w_v[...].astype(BF16)
         to_all(W.at[c, i, o], w1_s, w1_r, inner)
 
-    def weight_2():
-        settle(seven, w1_r)
-
-        def send(k, _):
-            row = W.at[c, :, o]
-            remote(row, row, w2_s.at[k], w2_r.at[k], outer(rem(k + 3, N - 1) + 1)).start()
-            return 0
-
-        lax.fori_loop(0, N - 1, send, 0)
+    def weight_2(n):
+        def go(ref, up):
+            remote(ref, ref, w2_s, w2_r.at[up, n], outer(1 if up else N - 1)).start()
+
+        if n == 0:
+            settle(seven, w1_r)
+            go(W.at[c, :, o], 1)
+            go(W.at[c, :, o], 0)
+            return
+        below, above = W.at[c, :, rem(o + N - n, N)], W.at[c, :, rem(o + n, N)]
+        settle(below, w2_r.at[1, n - 1])
+        if n < 4:
+            go(below, 1)
+            settle(above, w2_r.at[0, n - 1])
+        if n < 3:
+            go(above, 0)
 
     def weight_3():
-        def arrive(k, _):
-            settle(W.at[c, :, o], w2_r.at[k])
-            return 0
-
-        lax.fori_loop(0, N - 1, arrive, 0)
         remote(W.at[c], W.at[c], w3_s, w3_r, partner).start()
 
     def product(cot, rnn):
@@ -141,11 +156,8 @@
         part_in[j] = both
         rs1_out[j] = both.astype(BF16)
 
-        def send(k, _):
+        for k in FAR_FIRST:
             remote(rs1_out.at[j, rem(o + k, N)], rs1_in.at[j, k - 1], rs1_s.at[j], rs1_r.at[j], outer(k)).start()
-            return 0
-
-        lax.fori_loop(1, N, send, 0)
 
     def scatter_2(j):
         settle(seven, rs1_r.at[j])
@@ -155,20 +167,18 @@
         mine = total.astype(BF16)
         if (j // 2) % 2 == 1:
             ar_out[j] = mine
-
-            def send(k, _):
+            for k in FAR_FIRST + (0,):
                 remote(ar_out.at[j], ar_in.at[j, i], ar_s.at[j], ar_r.at[j], inner(k, x_rnn)).start()
-                return 0
-
-            lax.fori_loop(0, N, send, 0)
         else:
             ar_in[j, i] = mine
             to_all(ar_in.at[j, i], ar_s.at[j], ar_r.at[j], inner)
 
-    def g_piece(j):
-        return G.at[blocks[j // 2], j % 2, c, o]
-
-    def gather_2(j):
+    def g_sems(j):
+        return (
+            lambda s: G.at[blocks[j // 2], j % 2, c, s], g2_s.at[j], lambda k: g2_r.at[j], g2_up.at[j], g2_down.at[j]
+        )
+
+    def gather_1(j):
         settle(ar_in.at[j] if (j // 2) % 2 == 1 else seven, ar_r.at[j])
         piece = ar_in[j, 0].astype(F32)
         for s in range(1, N):
@@ -179,24 +189,37 @@
         def _():
             piece_v[...] = piece
 
-        to_all(g_piece(j), g2_s.at[j], g2_r.at[j], outer)
+        if j in LAST:
+            to_all(G.at[blocks[j // 2], j % 2, c, o], g2_s.at[j], g2_r.at[j], outer)
+        else:
+            spread(*g_sems(j))
+
+    def gather_2(j):
+        relay(*g_sems(j), j % 2 == 0)
 
     def gather_3(j):
-        settle(seven, g2_r.at[j])
+        settle(seven if j in LAST else five, g2_r.at[j])
         both = G.at[blocks[j // 2], j % 2, c]
         remote(both, both, g3_s, g3_r, partner).start()
 
-    weight_1()
     compute(0)
     compute(1)
+    learned(0, 4)
+    learn(1, (outer(2), outer(N - 2), inner(2), inner(N - 2)))
+    learned(1, 4)
+    learn(2, ((z, y, c, x_rnn),))
+    weight_1()
     scatter_1(0)
     scatter_1(1)
-    weight_2()
+    learned(2, 1)
+    learn(3, (partner,))
+    weight_2(0)
     x_copies[0].wait_recv()
     compute(4)
     scatter_2(0)
     scatter_2(1)
     scatter_1(4)
+    weight_2(1)
     x_copies[2].wait_recv()
     compute(2)
     compute(3)
@@ -204,28 +227,36 @@
     scatter_1(2)
     scatter_1(3)
     scatter_1(6)
-    gather_2(0)
-    gather_2(1)
-    scatter_2(4)
+    learned(3, 1)
     x_copies[1].wait_recv()
     compute(5)
     compute(7)
+    gather_1(0)
+    gather_1(1)
     scatter_1(5)
     scatter_1(7)
+    scatter_2(4)
+    weight_2(2)
+    gather_2(0)
+    gather_2(1)
     scatter_2(2)
     scatter_2(3)
     scatter_2(6)
-    gather_2(4)
+    gather_1(4)
     scatter_2(5)
     scatter_2(7)
+    gather_1(2)
+    gather_1(3)
+    gather_1(6)
+    gather_2(4)
+    gather_3(0)
+    gather_3(1)
+    gather_1(5)
+    gather_1(7)
     gather_2(2)
     gather_2(3)
     gather_2(6)
-    gather_3(0)
-    gather_3(1)
-    weight_3()
-    gather_2(5)
-    gather_2(7)
+    weight_2(3)
     gather_3(4)
     gather_3(2)
     gather_3(3)
@@ -241,21 +272,34 @@
     A[c, i, o] = rows
     to_all(A.at[c, i, o], a1_s, a1_r.at[i], inner)
 
+    def a_sems(n):
+        half = (n + 1) // 2
+        j = rem(i + half + ((n + 1) % 2) * (N - 2 * half), N)
+        return lambda s: A.at[c, j, s], a2_s, lambda k: a2_r.at[k], a2_up.at[j], a2_down.at[j], a1_r.at[j]
+
+    def applied_2(n):
+        *sems, arrival = a_sems(n)
+        if n:
+            settle(sems[0](o), arrival)
+        spread(sems[0], sems[1].at[0], *sems[2:])
+
+    def applied_3(n):
+        at, s, *sems, _ = a_sems(n)
+        relay(at, s.at[0], *sems, n % 2 == 0)
+
+    applied_2(0)
+
     update = jnp.dot(rows, rroot[...], preferred_element_type=F32)
     own_update[...] = update
     line = lax.broadcasted_iota(jnp.int32, (8, 128), 0)
     t1[o] = jnp.where(line == 0, jnp.sum(piece_v[...] * piece_v[...]), jnp.sum(update * update))
     to_all(t1.at[o], t_s.at[0], t_r.at[0], outer)
-    to_all(A.at[c, i, o], a2_s.at[i], a2_r.at[i], outer)
-
-    def relay(k, _):
-        half = (k + 1) // 2
-        j = rem(i + half + rem(k + 1, 2) * (N - 2 * half), N)
-        settle(A.at[c, j, o], a1_r.at[j])
-        to_all(A.at[c, j, o], a2_s.at[j], a2_r.at[j], outer)
-        return 0
-
-    lax.fori_loop(1, 5, relay, 0)
+
+    applied_2(1)
+    applied_2(2)
+    applied_3(0)
+    for n in range(3, N):
+        applied_2(n)
 
     def total_of(ref, count):
         total = ref[0]
@@ -266,7 +310,6 @@
     settle(t1.at[pl.ds(0, N - 1)], t_r.at[0])
     t2[i] = total_of(t1, N)
     to_all(t2.at[i], t_s.at[1], t_r.at[1], inner)
-    lax.fori_loop(5, N, relay, 0)
 
     index = (z * N + y) * 2 + c
     own = G[z // 2, rem(z, 2), y // 4, rem(y, 4) * 2 + c]
@@ -280,62 +323,68 @@
     for r in range(3):
         right_v[r] = decay_rate * rstat[r] + (1.0 - decay_rate) * (right_sum[r:r + 1] / 2048)
 
+    weight_2(4)
+    for n in range(1, N):
+        applied_3(n)
+    remote(A.at[c, :, o], A.at[c, :, o], a3_s, a3_r.at[0], partner).start()
+
+    weight_3()
+
+    def multiply(core, rows_of):
+        for s in rows_of:
+            upd[core, :, s] = jnp.dot(
+                A[core, :, s].reshape(128, 384), rroot[...], preferred_element_type=F32
+            ).reshape(N, 16, 384)
+
+    def source(k):
+        return rem(o - k + N, N)
+
+    def partner_source(k):
+        return rem(i - k + N, N)
+
+    def pass_on(k):
+        s = source(k)
+        if k not in (2, N - 2):
+            settle(A.at[c, :, s], a2_r.at[k])
+        remote(A.at[c, :, s], A.at[c, :, s], a3_s, a3_r.at[k], partner).start()
+
+    def take(k):
+        settle(A.at[1 - c, :, partner_source(k)], a3_r.at[k])
+
+    def finish(core, rows_of):
+        for s in rows_of:
+            for t in range(N):
+                value = W[core, t, s].astype(F32) - step_size * (scale * upd[core, t, s])
+                wc_v[t + core * (s - t), s + core * (t - s), core] = value.astype(BF16)
+
+    early, late = (0, 2, 6, 1, 7), (3, 5, 4)
+    pass_on(2)
+    pass_on(6)
     settle(t2.at[pl.ds(0, N - 1)], t_r.at[1])
-    t3[...] = total_of(t2, N)
-    remote(t3, t3_in, t_s.at[2], t_r.at[2], partner).start()
-
-    def pass_on(k):
-        j = near(i, k)
-        settle(seven, a2_r.at[j])
-        remote(A.at[c, j], A.at[c, j], a3_s, a3_r.at[j], partner).start()
-        multiply(c, j)
-
-    def near(start, k):
-        half = (k + 1) // 2
-        return rem(start + half + ((k + 1) % 2) * (N - 2 * half), N)
-
-    def multiply(core, j):
-        upd[core, j] = jnp.dot(
-            A[core, j].reshape(128, 384), rroot[...], preferred_element_type=F32
-        ).reshape(N, 16, 384)
-
-    def take(k):
-        j = near(o, k)
-        settle(A.at[c, j], a3_r.at[j])
-        multiply(1 - c, j)
-
-    pass_on(0)
+    t3[c, x] = total_of(t2, N)
+    to_all(t3.at[c, x], t_s.at[2], t_r.at[2], chip_x)
     pass_on(1)
-    pass_on(2)
-    settle(t3, t_r.at[2])
-    t4[x] = t3[...] + t3_in[...]
-    to_all(t4.at[x], t_s.at[3], t_r.at[3], along_x, 4)
-    pass_on(3)
-    take(0)
-    pass_on(4)
-    take(1)
-    take(2)
-    pass_on(5)
-    take(3)
-    pass_on(6)
-    take(4)
     pass_on(7)
-    take(5)
+    multiply(c, [source(k) for k in early])
+    for k in early:
+        take(k)
+    multiply(1 - c, [partner_source(k) for k in early])
+    for k in late:
+        pass_on(k)
+    multiply(c, [source(k) for k in late])
     settle(W.at[1 - c], w3_r)
-    settle(t4.at[pl.ds(0, 3)], t_r.at[3])
-    sums = total_of(t4, 4)
+    settle(t1.at[pl.ds(0, N - 1)], t_r.at[2])
+    sums = total_of(t3[0] + t3[1], 4)
     scale = jnp.sqrt(sums[0:1, 0:1] + 1.0) / jnp.sqrt(sums[1:2, 0:1] + 1.0)
     step = scale * own_update[...]
     step_v[...] = step
     nw_v[...] = w_v[...] - step_size * step
-    take(6)
-    take(7)
-    for oo in range(N):
-        for ii in range(N):
-            first = W[0, ii, oo].astype(F32) - step_size * (scale * upd[0, ii, oo])
-            wc_v[ii, oo, 0] = first.astype(BF16)
-            second = W[1, ii, oo].astype(F32) - step_size * (scale * upd[1, ii, oo])
-            wc_v[oo, ii, 1] = second.astype(BF16)
+    finish(c, [source(k) for k in early + late])
+    finish(1 - c, [partner_source(k) for k in early])
+    for k in late:
+        take(k)
+    multiply(1 - c, [partner_source(k) for k in late])
+    finish(1 - c, [partner_source(k) for k in late])
 
     for n in range(3):
         x_copies[n].wait_send()
@@ -343,22 +392,17 @@
         d2d(j).wait_send()
         settle(seven, rs1_s.at[j])
         settle(seven, g2_s.at[j])
-        settle(seven, a2_s.at[j])
         settle(ar_in.at[j] if (j // 2) % 2 == 1 else seven, ar_s.at[j])
 
-    def sent(k, _):
-        settle(W.at[c, :, o], w2_s.at[k])
-        return 0
-
-    lax.fori_loop(0, N - 1, sent, 0)
+    settle(W.at[c, :, pl.ds(0, N - 1)], w2_s)
     settle(seven, a1_s)
+    settle(A.at[c, pl.ds(0, N - 1)], a2_s.at[0])
     settle(seven, w1_s)
     for sem in (g3_s, a3_s, w3_s):
         settle(W.at[c], sem)
     settle(t1.at[pl.ds(0, N - 1)], t_s.at[0])
     settle(t2.at[pl.ds(0, N - 1)], t_s.at[1])
-    settle(t3, t_s.at[2])
-    settle(t4.at[pl.ds(0, 3)], t_s.at[3])
+    settle(t1.at[pl.ds(0, N - 1)], t_s.at[2])
 
 
 def write(*refs):
@@ -391,11 +435,12 @@
             v((N, 16, 384), BF16), v((N, N, 16, 384), BF16),
             v((4, 2, 2, N, 16, 384), BF16), v((2, N, N, 16, 384), BF16), v((2, N, N, 16, 384), BF16),
             v((2, N, N, 16, 384), F32), v((16, 384), F32), v((16, 384), F32),
-            v((N, 8, 128), F32), v((N, 8, 128), F32), v((8, 128), F32), v((8, 128), F32), v((4, 8, 128), F32),
-            dma((7,)),
+            v((N, 8, 128), F32), v((N, 8, 128), F32), v((2, 4, 8, 128), F32),
+            dma((7,)), pltpu.SemaphoreType.REGULAR((4,)),
             dma((3,)), dma((3,)), dma((N,)), dma((N,)), dma((N,)), dma((N,)), dma((N,)), dma((N,)),
-            dma((N,)), dma((N,)), dma, dma, dma, dma((N,)), dma((N,)), dma((N,)), dma, dma((N,)),
-            dma, dma, dma((N - 1,)), dma((N - 1,)), dma, dma, dma((4,)), dma((4,)),
+            dma((N,)), dma((N,)), dma((N,)), dma((N,)), dma, dma,
+            dma, dma((N,)), dma((N,)), dma((N,)), dma((N,)), dma((N,)), dma, dma((N,)),
+            dma, dma, dma, dma((2, 4)), dma, dma, dma((3,)), dma((3,)),
         ],
         compiler_params=pltpu.CompilerParams(collective_id=0, has_side_effects=True),
     )(rnn_out, out_grad, weight, left_root[0], right_root[0], left_stat[0], jnp.transpose(right_stat, (1, 0, 2)))

time: 81.1 us -> 75.4 us (0.930)
  Pallas kernels: 80.3 us -> 74.6 us
    pallas_call x1, Pallas kernels: 79.1 us -> 73.4 us  [body(): pl.pallas_call(kernel, name='step', out_shape=tuple((pltpu.VMEM(*shape) f...]
where the time goes in v3:
time: 75.4 us; the launch traced here: 75.3 us
  Pallas kernels  74.6 us (99%)
    pallas_call x1, Pallas kernels, body(): pl.pallas_call(kernel, name='step', out_shape=tuple((pltpu.VMEM(*shape) f...  73.4 us

profile of v3, /device:TPU:1, one launch (start us, length us, event | category | flops | bytes accessed | tf_op | source)
XLA Modules:
  0.0 75.3 jit_solution(134488786940577184)
XLA Ops:
  0.6 73.4 %step.1 = (f32[16,384]{1,0:T(8,128)S(1)}, f32[16,384]{1,0:T(8,128)S(1)}, f32[16,2048]{1,0:T(8,128)S(1)}, f32[3,1,384]{2,1,0:T(1,128)S(1)}, bf16[8,8,2,16,384]{4,3,2,1,0:T(8,128)(2,1)S(1)}) custom-call(bf16[768,384]{1,0:T(8,128)(2,1)} %rnn_hbm.1, bf16[768,512]{1,0:T(8,128)(2,1)} %cot_hbm.1, f32[16,384]{1,0:T(8,128)} %w_hbm.1, bf16[16,2048]{1,0:T(8,128)(2,1)} %bitcast.9, ...), custom_call_target="tpu_custom_call" | custom-call | tf_op jit(solution)/shard_map/step/pallas_call | solution.py:424
  74.1 1.2 %write.1 = (f32[16,384]{1,0:T(8,128)}, f32[16,384]{1,0:T(8,128)}, f32[16,2048]{1,0:T(8,128)}, f32[3,1,384]{2,1,0:T(1,128)}, bf16[8,8,2,16,384]{4,3,2,1,0:T(8,128)(2,1)}) custom-call(f32[16,384]{1,0:T(8,128)S(1)} %get-tuple-element.15.refs_0_, f32[16,384]{1,0:T(8,128)S(1)} %get-tuple-element.16.refs_1_, f32[16,2048]{1,0:T(8,128)S(1)} %get-tuple-element.17.refs_2_, ...), custom_call_target="tpu_custom_call" | custom-call | tf_op jit(solution)/shard_map/write/pallas_call | solution.py:447

commit v4 on v3

--- a/solution.py
+++ b/solution.py
@@ -19,6 +19,7 @@
 
 
 LAST = (5, 7)
+RELAYED = 8
 FAR_FIRST = (4, 5, 3, 6, 2, 7, 1)
 
 
@@ -46,9 +47,6 @@
     def inner(k, xx=None):
         return (rem(z + (1 - c) * k, N), rem(y + c * k, N), c, x if xx is None else xx)
 
-    def chip_x(k):
-        return (z, y, rem(c + k // 4, 2), rem(x + k, 4))
-
     partner = (z, y, 1 - c, x)
 
     def remote(src, dst, s, r, to):
@@ -65,6 +63,7 @@
 
     seven = rs1_in.at[0]
     five = rs1_in.at[0, pl.ds(0, 5)]
+    thirty_one = t2.at[pl.ds(0, 4 * N - 1)]
     def spread(at, s, r, up, down):
         for k, sem in ((2, up), (N - 2, down), (1, r(1)), (N - 1, r(N - 1))):
             remote(at(o), at(o), s, sem, outer(k)).start()
@@ -207,12 +206,12 @@
     learned(0, 4)
     learn(1, (outer(2), outer(N - 2), inner(2), inner(N - 2)))
     learned(1, 4)
-    learn(2, ((z, y, c, x_rnn),))
+    learn(2, ((z, y, c, x_rnn), (z, y, c, x_cot)))
     weight_1()
     scatter_1(0)
     scatter_1(1)
-    learned(2, 1)
-    learn(3, (partner,))
+    learned(2, 2)
+    learn(3, ((z, y, c, x_rnn), partner))
     weight_2(0)
     x_copies[0].wait_recv()
     compute(4)
@@ -227,7 +226,7 @@
     scatter_1(2)
     scatter_1(3)
     scatter_1(6)
-    learned(3, 1)
+    learned(3, 2)
     x_copies[1].wait_recv()
     compute(5)
     compute(7)
@@ -237,11 +236,11 @@
     scatter_1(7)
     scatter_2(4)
     weight_2(2)
-    gather_2(0)
-    gather_2(1)
     scatter_2(2)
     scatter_2(3)
     scatter_2(6)
+    gather_2(0)
+    gather_2(1)
     gather_1(4)
     scatter_2(5)
     scatter_2(7)
@@ -281,19 +280,31 @@
         *sems, arrival = a_sems(n)
         if n:
             settle(sems[0](o), arrival)
-        spread(sems[0], sems[1].at[0], *sems[2:])
+        if n < RELAYED:
+            spread(sems[0], sems[1].at[0], *sems[2:])
+        else:
+            at, s, r, up, down = sems
+            for k in FAR_FIRST:
+                sem = {2: up, N - 2: down}.get(k)
+                remote(at(o), at(o), s.at[0], r(k) if sem is None else sem, outer(k)).start()
 
     def applied_3(n):
         at, s, *sems, _ = a_sems(n)
-        relay(at, s.at[0], *sems, n % 2 == 0)
+        if n < RELAYED:
+            relay(at, s.at[0], *sems, n % 2 == 0)
+        else:
+            settle(at(rem(o + N - 2, N)), sems[1])
+            settle(at(rem(o + 2, N)), sems[2])
 
     applied_2(0)
 
     update = jnp.dot(rows, rroot[...], preferred_element_type=F32)
     own_update[...] = update
-    line = lax.broadcasted_iota(jnp.int32, (8, 128), 0)
-    t1[o] = jnp.where(line == 0, jnp.sum(piece_v[...] * piece_v[...]), jnp.sum(update * update))
+    lane = lax.broadcasted_iota(jnp.int32, (1, 128), 1)
+    t1[o] = jnp.where(lane == 0, jnp.sum(piece_v[...] * piece_v[...]), jnp.sum(update * update))
     to_all(t1.at[o], t_s.at[0], t_r.at[0], outer)
+    weight_2(4)
+    weight_3()
 
     applied_2(1)
     applied_2(2)
@@ -308,8 +319,13 @@
         return total
 
     settle(t1.at[pl.ds(0, N - 1)], t_r.at[0])
-    t2[i] = total_of(t1, N)
-    to_all(t2.at[i], t_s.at[1], t_r.at[1], inner)
+    mine = N * x + i
+    t2[mine] = total_of(t1, N)
+    for k in FAR_FIRST:
+        for away in (2, 1, 3, 0):
+            remote(t2.at[mine], t2.at[mine], t_s.at[1], t_r.at[1], inner(k, rem(x + away, 4))).start()
+    for away in (2, 1, 3):
+        remote(t2.at[mine], t2.at[mine], t_s.at[1], t_r.at[1], (z, y, c, rem(x + away, 4))).start()
 
     index = (z * N + y) * 2 + c
     own = G[z // 2, rem(z, 2), y // 4, rem(y, 4) * 2 + c]
@@ -323,12 +339,9 @@
     for r in range(3):
         right_v[r] = decay_rate * rstat[r] + (1.0 - decay_rate) * (right_sum[r:r + 1] / 2048)
 
-    weight_2(4)
     for n in range(1, N):
         applied_3(n)
     remote(A.at[c, :, o], A.at[c, :, o], a3_s, a3_r.at[0], partner).start()
-
-    weight_3()
 
     def multiply(core, rows_of):
         for s in rows_of:
@@ -360,9 +373,9 @@
     early, late = (0, 2, 6, 1, 7), (3, 5, 4)
     pass_on(2)
     pass_on(6)
-    settle(t2.at[pl.ds(0, N - 1)], t_r.at[1])
-    t3[c, x] = total_of(t2, N)
-    to_all(t3.at[c, x], t_s.at[2], t_r.at[2], chip_x)
+    settle(thirty_one, t_r.at[1])
+    t3[c] = total_of(t2, 4 * N)
+    remote(t3.at[c], t3.at[c], t_s.at[2], t_r.at[2], partner).start()
     pass_on(1)
     pass_on(7)
     multiply(c, [source(k) for k in early])
@@ -373,9 +386,9 @@
         pass_on(k)
     multiply(c, [source(k) for k in late])
     settle(W.at[1 - c], w3_r)
-    settle(t1.at[pl.ds(0, N - 1)], t_r.at[2])
-    sums = total_of(t3[0] + t3[1], 4)
-    scale = jnp.sqrt(sums[0:1, 0:1] + 1.0) / jnp.sqrt(sums[1:2, 0:1] + 1.0)
+    settle(t3.at[0], t_r.at[2])
+    sums = t3[0] + t3[1]
+    scale = jnp.sqrt(sums[0:1, 0:1] + 1.0) / jnp.sqrt(sums[0:1, 1:2] + 1.0)
     step = scale * own_update[...]
     step_v[...] = step
     nw_v[...] = w_v[...] - step_size * step
@@ -401,8 +414,8 @@
     for sem in (g3_s, a3_s, w3_s):
         settle(W.at[c], sem)
     settle(t1.at[pl.ds(0, N - 1)], t_s.at[0])
-    settle(t2.at[pl.ds(0, N - 1)], t_s.at[1])
-    settle(t1.at[pl.ds(0, N - 1)], t_s.at[2])
+    settle(thirty_one, t_s.at[1])
+    settle(t3.at[0], t_s.at[2])
 
 
 def write(*refs):
@@ -435,7 +448,7 @@
             v((N, 16, 384), BF16), v((N, N, 16, 384), BF16),
             v((4, 2, 2, N, 16, 384), BF16), v((2, N, N, 16, 384), BF16), v((2, N, N, 16, 384), BF16),
             v((2, N, N, 16, 384), F32), v((16, 384), F32), v((16, 384), F32),
-            v((N, 8, 128), F32), v((N, 8, 128), F32), v((2, 4, 8, 128), F32),
+            v((N, 1, 128), F32), v((4 * N, 1, 128), F32), v((2, 1, 128), F32),
             dma((7,)), pltpu.SemaphoreType.REGULAR((4,)),
             dma((3,)), dma((3,)), dma((N,)), dma((N,)), dma((N,)), dma((N,)), dma((N,)), dma((N,)),
             dma((N,)), dma((N,)), dma((N,)), dma((N,)), dma, dma,

time: 75.4 us -> 74 us (0.981)
  Pallas kernels: 74.6 us -> 73.3 us
    pallas_call x1, Pallas kernels: 73.4 us -> 72 us  [body(): pl.pallas_call(kernel, name='step', out_shape=tuple((pltpu.VMEM(*shape) f...]
where the time goes in v4:
time: 74 us; the launch traced here: 73.9 us
  Pallas kernels  73.3 us (99%)
    pallas_call x1, Pallas kernels, body(): pl.pallas_call(kernel, name='step', out_shape=tuple((pltpu.VMEM(*shape) f...  72 us

profile of v4, /device:TPU:1, one launch (start us, length us, event | category | flops | bytes accessed | tf_op | source)
XLA Modules:
  0.0 73.9 jit_solution(3657640569628357793)
XLA Ops:
  0.6 72.0 %step.1 = (f32[16,384]{1,0:T(8,128)S(1)}, f32[16,384]{1,0:T(8,128)S(1)}, f32[16,2048]{1,0:T(8,128)S(1)}, f32[3,1,384]{2,1,0:T(1,128)S(1)}, bf16[8,8,2,16,384]{4,3,2,1,0:T(8,128)(2,1)S(1)}) custom-call(bf16[768,384]{1,0:T(8,128)(2,1)} %rnn_hbm.1, bf16[768,512]{1,0:T(8,128)(2,1)} %cot_hbm.1, f32[16,384]{1,0:T(8,128)} %w_hbm.1, bf16[16,2048]{1,0:T(8,128)(2,1)} %bitcast.9, ...), custom_call_target="tpu_custom_call" | custom-call | tf_op jit(solution)/shard_map/step/pallas_call | solution.py:437
  72.7 1.2 %write.1 = (f32[16,384]{1,0:T(8,128)}, f32[16,384]{1,0:T(8,128)}, f32[16,2048]{1,0:T(8,128)}, f32[3,1,384]{2,1,0:T(1,128)}, bf16[8,8,2,16,384]{4,3,2,1,0:T(8,128)(2,1)}) custom-call(f32[16,384]{1,0:T(8,128)S(1)} %get-tuple-element.15.refs_0_, f32[16,384]{1,0:T(8,128)S(1)} %get-tuple-element.16.refs_1_, f32[16,2048]{1,0:T(8,128)S(1)} %get-tuple-element.17.refs_2_, ...), custom_call_target="tpu_custom_call" | custom-call | tf_op jit(solution)/shard_map/write/pallas_call | solution.py:460

commit v5 on v4

--- a/solution.py
+++ b/solution.py
@@ -327,6 +327,47 @@
     for away in (2, 1, 3):
         remote(t2.at[mine], t2.at[mine], t_s.at[1], t_r.at[1], (z, y, c, rem(x + away, 4))).start()
 
+    for n in range(1, N):
+        applied_3(n)
+    remote(A.at[c, :, o], A.at[c, :, o], a3_s, a3_r.at[0], partner).start()
+
+    def multiply(core, rows_of):
+        for s in rows_of:
+            upd[core, :, s] = jnp.dot(
+                A[core, :, s].reshape(128, 384), rroot[...], preferred_element_type=F32
+            ).reshape(N, 16, 384)
+
+    def source(k):
+        return rem(o - k + N, N)
+
+    def partner_source(k):
+        return rem(i - k + N, N)
+
+    def pass_on(k):
+        s = source(k)
+        if k not in (2, N - 2):
+            settle(A.at[c, :, s], a2_r.at[k])
+        remote(A.at[c, :, s], A.at[c, :, s], a3_s, a3_r.at[k], partner).start()
+
+    def take(k):
+        settle(A.at[1 - c, :, partner_source(k)], a3_r.at[k])
+
+    def finish(core, rows_of):
+        for s in rows_of:
+            for t in range(N):
+                value = W[core, t, s].astype(F32) - step_size * (scale * upd[core, t, s])
+                wc_v[t + core * (s - t), s + core * (t - s), core] = value.astype(BF16)
+
+    early, late = (0, 2, 6, 1, 7), (3, 5, 4)
+    pass_on(2)
+    pass_on(6)
+    pass_on(1)
+    pass_on(7)
+    settle(thirty_one, t_r.at[1])
+    t3[c] = total_of(t2, 4 * N)
+    remote(t3.at[c], t3.at[c], t_s.at[2], t_r.at[2], partner).start()
+    multiply(c, [source(k) for k in early])
+
     index = (z * N + y) * 2 + c
     own = G[z // 2, rem(z, 2), y // 4, rem(y, 4) * 2 + c]
     outer_sum = lax.dot_general(own, grad, (((1,), (1,)), ((), ())), preferred_element_type=F32)
@@ -339,46 +380,6 @@
     for r in range(3):
         right_v[r] = decay_rate * rstat[r] + (1.0 - decay_rate) * (right_sum[r:r + 1] / 2048)
 
-    for n in range(1, N):
-        applied_3(n)
-    remote(A.at[c, :, o], A.at[c, :, o], a3_s, a3_r.at[0], partner).start()
-
-    def multiply(core, rows_of):
-        for s in rows_of:
-            upd[core, :, s] = jnp.dot(
-                A[core, :, s].reshape(128, 384), rroot[...], preferred_element_type=F32
-            ).reshape(N, 16, 384)
-
-    def source(k):
-        return rem(o - k + N, N)
-
-    def partner_source(k):
-        return rem(i - k + N, N)
-
-    def pass_on(k):
-        s = source(k)
-        if k not in (2, N - 2):
-            settle(A.at[c, :, s], a2_r.at[k])
-        remote(A.at[c, :, s], A.at[c, :, s], a3_s, a3_r.at[k], partner).start()
-
-    def take(k):
-        settle(A.at[1 - c, :, partner_source(k)], a3_r.at[k])
-
-    def finish(core, rows_of):
-        for s in rows_of:
-            for t in range(N):
-                value = W[core, t, s].astype(F32) - step_size * (scale * upd[core, t, s])
-                wc_v[t + core * (s - t), s + core * (t - s), core] = value.astype(BF16)
-
-    early, late = (0, 2, 6, 1, 7), (3, 5, 4)
-    pass_on(2)
-    pass_on(6)
-    settle(thirty_one, t_r.at[1])
-    t3[c] = total_of(t2, 4 * N)
-    remote(t3.at[c], t3.at[c], t_s.at[2], t_r.at[2], partner).start()
-    pass_on(1)
-    pass_on(7)
-    multiply(c, [source(k) for k in early])
     for k in early:
         take(k)
     multiply(1 - c, [partner_source(k) for k in early])
@@ -420,7 +421,8 @@
 
 def write(*refs):
     *refs, sem = refs
-    stores = [pltpu.make_async_copy(refs[n], refs[5 + n], sem.at[n]) for n in (4, 2, 0, 1, 3)]
+    pairs = [(refs[4].at[n], refs[9].at[n]) for n in range(N)] + [(refs[n], refs[5 + n]) for n in (2, 0, 1, 3)]
+    stores = [pltpu.make_async_copy(src, dst, sem.at[n]) for n, (src, dst) in enumerate(pairs)]
     for store in stores:
         store.start()
     for store in stores:
@@ -463,7 +465,7 @@
         out_shape=tuple(jax.ShapeDtypeStruct(*shape) for shape in outs),
         in_specs=[vmem] * 5,
         out_specs=(hbm,) * 5,
-        scratch_shapes=[dma((5,))],
+        scratch_shapes=[dma((N + 4,))],
     )(*(pltpu.with_memory_space_constraint(result, pltpu.VMEM) for result in results))
     return new_weight, step, left_new[None], jnp.transpose(right_new, (1, 0, 2)), copy.reshape(2048, 384)
 

time: 74 us -> 74.2 us (level)
  no operation moved by 1% of the time
where the time goes in v5:
time: 74.2 us; the launch traced here: 74.1 us
  Pallas kernels  73.4 us (99%)
    pallas_call x1, Pallas kernels, body(): pl.pallas_call(kernel, name='step', out_shape=tuple((pltpu.VMEM(*shape) f...  72.1 us

profile of v5, /device:TPU:1, one launch (start us, length us, event | category | flops | bytes accessed | tf_op | source)
XLA Modules:
  0.0 74.1 jit_solution(18316206749070295800)
XLA Ops:
  0.6 72.1 %step.1 = (f32[16,384]{1,0:T(8,128)S(1)}, f32[16,384]{1,0:T(8,128)S(1)}, f32[16,2048]{1,0:T(8,128)S(1)}, f32[3,1,384]{2,1,0:T(1,128)S(1)}, bf16[8,8,2,16,384]{4,3,2,1,0:T(8,128)(2,1)S(1)}) custom-call(bf16[768,384]{1,0:T(8,128)(2,1)} %rnn_hbm.1, bf16[768,512]{1,0:T(8,128)(2,1)} %cot_hbm.1, f32[16,384]{1,0:T(8,128)} %w_hbm.1, bf16[16,2048]{1,0:T(8,128)(2,1)} %bitcast.9, ...), custom_call_target="tpu_custom_call" | custom-call | tf_op jit(solution)/shard_map/step/pallas_call | solution.py:439
  72.8 1.3 %write.1 = (f32[16,384]{1,0:T(8,128)}, f32[16,384]{1,0:T(8,128)}, f32[16,2048]{1,0:T(8,128)}, f32[3,1,384]{2,1,0:T(1,128)}, bf16[8,8,2,16,384]{4,3,2,1,0:T(8,128)(2,1)}) custom-call(f32[16,384]{1,0:T(8,128)S(1)} %get-tuple-element.15.refs_0_, f32[16,384]{1,0:T(8,128)S(1)} %get-tuple-element.16.refs_1_, f32[16,2048]{1,0:T(8,128)S(1)} %get-tuple-element.17.refs_2_, ...), custom_call_target="tpu_custom_call" | custom-call | tf_op jit(solution)/shard_map/write/pallas_call | solution.py:462
